TPU v7x, 32 devices: a whole 2x2x4 slice. The times are simulated.
32 devices in a mesh: kv: 4 (over y, x), tp: 8 (over z, core).
Axes of the slice: x: 2, y: 2, z: 4, core: 2. Of those that a mesh axis runs over, the one named last changes fastest.
Arguments:
- tokens: bfloat16 [384, 4096], P('kv', 'tp'), may hold values from -20 to 20
- state: float32 [384, 32, 4096], P('kv', 'tp'), may hold values from -4 to 4
- w_query: bfloat16 [4096, 2048], P(None, 'tp'), may hold values from -0.09375 to 0.09375
- w_key: bfloat16 [4096, 2048], P(None, 'tp'), may hold values from -0.09375 to 0.09375
- w_value: bfloat16 [4096, 2048], P(None, 'tp'), may hold values from -0.09375 to 0.09375
- w_gate: bfloat16 [4096, 2048], P(None, 'tp'), may hold values from -0.09375 to 0.09375
- w_decay: bfloat16 [4096, 32], replicated, may hold values from -0.09375 to 0.09375
- w_beta: bfloat16 [4096, 32], replicated, may hold values from -0.09375 to 0.09375
- decay_rate: float32 [32], P('tp'), may hold values from 0.03 to 3
- decay_bias: float32 [32], P('tp'), may hold values from -1 to 1
- mix_gain: float32 [4096], replicated, may hold values from 0.1 to 1.9
- out_gain: float32 [64], replicated, may hold values from 0.1 to 1.9
- w_out: bfloat16 [2048, 4096], P('tp'), may hold values from -0.125 to 0.125
- ffn_gain: float32 [4096], replicated, may hold values from 0.1 to 1.9
- w_up: bfloat16 [4096, 16384], P('tp', 'kv'), may hold values from -0.09375 to 0.09375
- w_down: bfloat16 [16384, 4096], P('kv', 'tp'), may hold values from -0.046875 to 0.046875
Outputs:
- mixed: bfloat16 [384, 4096], P('kv', 'tp')
- new_state: float32 [384, 32, 4096], P('kv', 'tp')
All inputs are finite; a program needn't handle non-finite values.
Results may differ from a plain program's by a relative error of at most 0.024.
Values may be sent and summed in bfloat16 or wider, within the bound.
A program may use at most 128 MiB of HBM per device.

v0:
```python
import jax
import jax.numpy as jnp
from jax import lax
from jax.sharding import PartitionSpec as P

D = 4096
HEAD_DIM = 64
EPS = 1e-06


def unit_norm(vector):
    return vector * lax.rsqrt(jnp.sum(vector * vector, axis=-1, keepdims=True) + EPS)


def local(
    tokens,
    state,
    w_query,
    w_key,
    w_value,
    w_gate,
    w_decay,
    w_beta,
    decay_rate,
    decay_bias,
    mix_gain,
    out_gain,
    w_out,
    ffn_gain,
    w_up,
    w_down,
):
    rows = tokens.shape[0]
    width_share = tokens.shape[1]
    head_count = w_query.shape[1] // HEAD_DIM
    full_rows = lax.all_gather(tokens, "tp", axis=1, tiled=True)
    full_f = full_rows.astype(jnp.float32)
    normed = (
        full_f * lax.rsqrt(jnp.mean(full_f * full_f, axis=-1, keepdims=True) + EPS) * mix_gain
    ).astype(jnp.bfloat16)
    query = jnp.dot(normed, w_query, preferred_element_type=jnp.float32).reshape(
        rows, head_count, HEAD_DIM
    )
    key_proj = jnp.dot(normed, w_key, preferred_element_type=jnp.float32).reshape(
        rows, head_count, HEAD_DIM
    )
    value = jnp.dot(normed, w_value, preferred_element_type=jnp.float32).reshape(
        rows, head_count, HEAD_DIM
    )
    gate = jnp.dot(normed, w_gate, preferred_element_type=jnp.float32).reshape(
        rows, head_count, HEAD_DIM
    )
    query = unit_norm(query) * HEAD_DIM ** (-0.5)
    key_proj = unit_norm(key_proj)
    head_start = lax.axis_index("tp") * head_count
    decay_cols = lax.dynamic_slice_in_dim(w_decay, head_start, head_count, 1)
    beta_cols = lax.dynamic_slice_in_dim(w_beta, head_start, head_count, 1)
    pre_decay = jnp.dot(normed, decay_cols, preferred_element_type=jnp.float32)
    decay = jnp.exp(-decay_rate * jax.nn.softplus(pre_decay + decay_bias))
    strength = jax.nn.sigmoid(jnp.dot(normed, beta_cols, preferred_element_type=jnp.float32))
    matrix = state.reshape(rows, head_count, HEAD_DIM, HEAD_DIM) * decay[:, :, None, None]
    recalled = jnp.einsum("bhk,bhkv->bhv", key_proj, matrix, precision=lax.Precision.HIGHEST)
    delta = (value - recalled) * strength[:, :, None]
    matrix = matrix + key_proj[:, :, :, None] * delta[:, :, None, :]
    head_out = jnp.einsum("bhk,bhkv->bhv", query, matrix, precision=lax.Precision.HIGHEST)
    head_out = (
        head_out
        * lax.rsqrt(jnp.mean(head_out * head_out, axis=-1, keepdims=True) + EPS)
        * out_gain
        * jax.nn.silu(gate)
    )
    head_out = head_out.reshape(rows, head_count * HEAD_DIM).astype(jnp.bfloat16)
    partial_value = jnp.dot(head_out, w_out, preferred_element_type=jnp.float32)
    feature_start = lax.axis_index("tp") * width_share
    gain_share = lax.dynamic_slice_in_dim(ffn_gain, feature_start, width_share, 0)
    resid = tokens.astype(jnp.float32) + lax.psum_scatter(
        partial_value.astype(jnp.bfloat16), "tp", scatter_dimension=1, tiled=True
    ).astype(jnp.float32)
    squares = lax.psum(jnp.sum(resid * resid, axis=-1), "tp")
    scale = lax.rsqrt(squares[:, None] / D + EPS)
    ffn_in = (resid * scale * gain_share).astype(jnp.bfloat16)
    up_part = jnp.dot(
        lax.all_gather(ffn_in, "kv", axis=0, tiled=True), w_up, preferred_element_type=jnp.float32
    )
    up_full = lax.psum(up_part.astype(jnp.bfloat16), "tp").astype(jnp.float32)
    hidden = jnp.square(jax.nn.relu(up_full)).astype(jnp.bfloat16)
    down = lax.psum_scatter(
        jnp.dot(hidden, w_down, preferred_element_type=jnp.float32).astype(jnp.bfloat16),
        "kv",
        scatter_dimension=0,
        tiled=True,
    ).astype(jnp.float32)
    mixed = (resid + down).astype(jnp.bfloat16)
    return (mixed, matrix.reshape(rows, head_count, HEAD_DIM * HEAD_DIM))


def solution(mesh):
    in_specs = (
        P("kv", "tp"),
        P("kv", "tp", None),
        P(None, "tp"),
        P(None, "tp"),
        P(None, "tp"),
        P(None, "tp"),
        P(),
        P(),
        P("tp"),
        P("tp"),
        P(),
        P(),
        P("tp", None),
        P(),
        P("tp", "kv"),
        P("kv", "tp"),
    )
    out_specs = (P("kv", "tp"), P("kv", "tp", None))
    return jax.shard_map(local, mesh=mesh, in_specs=in_specs, out_specs=out_specs, check_vma=False)
```

profile of v0, /device:TPU:0, one launch (start us, length us, event | category | flops | bytes accessed | tf_op | source)
XLA Modules:
  0.0 233.8 jit_solution(16335360079471447695)
XLA Ops:
  7.2 0.0 copy-start
  7.2 0.0 reduce-scatter.3.cloned.1.call-start
  7.2 0.8 neg.14
  8.0 17.4 %all_gather.6 = bf16[96,4096]{1,0:T(8,128)(2,1)S(1)} all-gather(bf16[96,512]{1,0:T(8,128)(2,1)} %param.16), channel_id=1, replica_groups=mesh['kv'=4,'tp'=8] {'tp'}, dimensions={1}, use_global_device_ids=true | all-gather | bytes 884736 | tf_op jit(solution)/shard_map/all_gather | solution.py:36
  25.4 0.3 fusion.2
  25.7 2.7 %fusion.21 = f32[96,256]{0,1:T(8,128)S(1)} fusion(bf16[4096,256]{1,0:T(8,128)(2,1)} %param.20, bf16[96,4096]{1,0:T(8,128)(2,1)S(1)} %all_gather.6, f32[4096]{0:T(1024)} %param.26, f32[96]{0:T(128)S(1)} %add_rsqrt_fusion.4), kind=kOutput, calls=%fused_computation.45 | convolution fusion | flops 202899456 | bytes 2998656 | tf_op jit(solution)/shard_map/dot_general | solution.py:47
  28.4 0.0 copy-done.6
  28.4 0.0 copy-done.9
  28.4 0.0 copy-start.7
  28.5 1.0 fusion.18
  29.5 0.6 copy-done.7
  30.0 1.0 multiply_reduce_fusion.4
  31.1 0.6 copy-done.8
  31.6 1.0 multiply_reduce_fusion.5
  32.7 0.0 copy-start.10
  32.7 9.2 %copy.22 = f32[96,4,4096]{0,2,1:T(8,128)} copy(f32[96,4,4096]{2,1,0:T(4,128)} %param.17) | data formatting | bytes 12582912 | tf_op args[1]
  41.9 1.2 fusion.8
  43.1 0.0 copy-done.10
  43.1 1.2 fusion.12
  44.4 0.0 copy-start.2
  44.4 5.0 %multiply_reduce_fusion.1 = f32[96,4,64]{0,2,1:T(8,128)S(1)} fusion(f32[96,4,64,64]{0,3,2,1:T(8,128)} %bitcast.21, f32[96,4,64]{0,2,1:T(8,128)S(1)} %broadcast_multiply_fusion.1, f32[96,4]{0,1:T(4,128)S(1)} %fusion.12), kind=kLoop, calls=%fused_computation.2 | loop fusion | flops 4694016 | bytes 6489600 | tf_op jit(solution)/shard_map/bhk,bhkv->bhv/dot_general | solution.py:62
  49.5 0.7 copy-done.2
  50.2 4.2 %broadcast_multiply_fusion = (f32[96,4,64,64]{0,3,2,1:T(8,128)}, f32[96,4,64]{0,2,1:T(8,128)S(1)}) fusion(f32[96,4,64]{0,2,1:T(8,128)S(1)} %get-tuple-element.10, f32[96,4,64]{0,2,1:T(8,128)S(1)} %broadcast_multiply_fusion.1, f32[96,4,64,64]{0,3,2,1:T(8,128)S(1)} %bitcast.22, f32[96,4]{0,1:T(4,128)S(1)} %fusion.12, f32[96,4,64]{0,2,1:T(8,128)S(1)} %get-tuple-element.11), kind=kLoop, calls=%fused_computation.6 | loop fusion | flops 7839744 | bytes 12977664 | tf_op jit(solution)/shard_map/mul | solution.py:64
  54.4 0.0 copy-done.5
  54.4 0.1 multiply_convert_fusion.5
  54.5 0.0 copy-done
  54.5 1.4 convolution_convert_fusion.1
  55.9 0.0 reduce-scatter.3.cloned.1.call-update
  55.9 0.0 all-reduce.2.cloned.1.call-start
  56.0 0.8 dynamic_slice.11
  56.7 32.4 %reduce-scatter.3.cloned.1.call-done = bf16[96,512]{1,0:T(8,128)(2,1)} async-done(((bf16[96,4096]{1,0:T(8,128)(2,1)}), bf16[96,512]{1,0:T(8,128)(2,1)}) %reduce-scatter.3.cloned.1.call-update) | async-done | bytes 98320 | tf_op jit(solution)/shard_map/reduce_scatter | solution.py:76
  89.2 0.0 copy-done.3
  89.2 1.0 multiply_reduce_fusion.2
  90.2 13.8 %psum.14 = f32[96]{0:T(128)S(1)} all-reduce(f32[96]{0:T(128)S(1)} %multiply_reduce_fusion.2), channel_id=1, replica_groups=mesh['kv'=4,'tp'=8] {'tp'}, use_global_device_ids=true, to_apply=%region_6.7 | all-reduce | flops 96 | bytes 768 | tf_op jit(solution)/shard_map/psum | solution.py:79
  104.0 1.0 multiply_convert_fusion.4
  105.0 10.1 %all_gather.7 = bf16[384,512]{1,0:T(8,128)(2,1)S(1)} all-gather(bf16[96,512]{1,0:T(8,128)(2,1)S(1)} %multiply_convert_fusion.4), channel_id=1, replica_groups=mesh['kv'=4,'tp'=8] {'kv'}, dimensions={0}, use_global_device_ids=true | all-gather | bytes 491520 | tf_op jit(solution)/shard_map/all_gather | solution.py:83
  115.0 5.7 %convolution_convert_fusion = bf16[384,4096]{1,0:T(8,128)(2,1)} fusion(bf16[384,512]{1,0:T(8,128)(2,1)S(1)} %all_gather.7, bf16[512,4096]{1,0:T(8,128)(2,1)} %param.30), kind=kOutput, calls=%fused_computation.4 | convolution fusion | flops 1612185600 | bytes 7733248 | tf_op jit(solution)/shard_map/dot_general | solution.py:82
  120.7 0.0 all-reduce.2.cloned.1.call-update
  120.7 0.2 reduce-scatter.5.cloned.1.call-start
  120.9 74.3 %all-reduce.2.cloned.1.call-done = bf16[384,4096]{1,0:T(8,128)(2,1)} async-done(((bf16[384,4096]{1,0:T(8,128)(2,1)}), bf16[384,4096]{1,0:T(8,128)(2,1)}) %all-reduce.2.cloned.1.call-update) | async-done | bytes 3145744 | tf_op jit(solution)/shard_map/psum | solution.py:85
  195.2 5.7 %fusion.5 = bf16[384,512]{1,0:T(8,128)(2,1)} fusion(bf16[4096,512]{1,0:T(8,128)(2,1)} %param.31, bf16[384,4096]{1,0:T(8,128)(2,1)} %all-reduce.2.cloned.1.call-done), kind=kOutput, calls=%fused_computation.14 | convolution fusion | flops 1617100800 | bytes 7733248 | tf_op jit(solution)/shard_map/dot_general | solution.py:88
  200.9 0.0 reduce-scatter.5.cloned.1.call-update
  200.9 9.8 %bitcast_add_fusion = f32[96,4,4096]{0,2,1:T(8,128)} fusion(f32[96,4,64,64]{0,3,2,1:T(8,128)} %get-tuple-element.4, f32[96,4,4096]{0,2,1:T(8,128)} %copy.22, f32[96,4]{0,1:T(4,128)S(1)} %fusion.12), kind=kLoop, calls=%fused_computation | loop fusion | flops 3145728 | bytes 18875904 | tf_op jit(solution)/shard_map/add | solution.py:64
  210.7 9.6 %copy.27 = f32[96,4,4096]{2,1,0:T(4,128)} copy(f32[96,4,4096]{0,2,1:T(8,128)} %bitcast_add_fusion) | data formatting | bytes 12582912
  220.3 5.4 %reduce-scatter.5.cloned.1.call-done = bf16[96,512]{1,0:T(8,128)(2,1)} async-done(((bf16[384,512]{1,0:T(8,128)(2,1)}), bf16[96,512]{1,0:T(8,128)(2,1)}) %reduce-scatter.5.cloned.1.call-update) | async-done | bytes 98320 | tf_op jit(solution)/shard_map/reduce_scatter | solution.py:87
  225.7 0.0 copy-done.4
  225.7 1.6 add_convert_fusion
  227.3 0.0 copy-done.1
  (15 shorter events, 0.1 us)
Async XLA Ops:
  7.2 47.3 %copy-start = (bf16[256,4096]{1,0:T(8,128)(2,1)S(1)}, bf16[256,4096]{1,0:T(8,128)(2,1)}, u32[]{:S(2)}) copy-start(bf16[256,4096]{1,0:T(8,128)(2,1)} %param.28) | copy-start | bytes 6291460
  7.2 82.0 %reduce-scatter.3.cloned.1.call-start = ((), (), s32[]{:S(2)}) async-start(), calls=%async_computation.2 | async-start | bytes 884736 | tf_op jit(solution)/shard_map/reduce_scatter | solution.py:76
  25.4 3.0 %copy-start.6 = (bf16[4096,256]{1,0:T(8,128)(2,1)S(1)}, bf16[4096,256]{1,0:T(8,128)(2,1)}, u32[]{:S(2)}) copy-start(bf16[4096,256]{1,0:T(8,128)(2,1)} %param.21) | copy-start | bytes 6291460
  25.4 3.0 %copy-start.9 = (f32[4096]{0:T(1024)S(1)}, f32[4096]{0:T(1024)}, u32[]{:S(2)}) copy-start(f32[4096]{0:T(1024)} %param.26) | copy-start | bytes 49156
  28.4 1.6 copy-start.7
  30.0 1.6 copy-start.8
  32.7 10.4 %copy-start.10 = (f32[4]{0:T(128)S(1)}, f32[4]{0:T(128)}, u32[]{:S(2)}) copy-start(f32[4]{0:T(128)} %param.25) | copy-start | bytes 52
  44.4 5.8 %copy-start.2 = (f32[96,4,4096]{0,2,1:T(8,128)S(1)}, f32[96,4,4096]{0,2,1:T(8,128)}, u32[]{:S(2)}) copy-start(f32[96,4,4096]{0,2,1:T(8,128)} %copy.22) | copy-start | bytes 18874372
  50.2 4.2 %copy-start.5 = (f32[64]{0:T(128)S(1)}, f32[64]{0:T(128)}, u32[]{:S(2)}) copy-start(f32[64]{0:T(128)} %param.27) | copy-start | bytes 772
  54.4 34.8 %copy-start.3 = (bf16[96,512]{1,0:T(8,128)(2,1)S(1)}, bf16[96,512]{1,0:T(8,128)(2,1)}, u32[]{:S(2)}) copy-start(bf16[96,512]{1,0:T(8,128)(2,1)} %param.16) | copy-start | bytes 294916
  55.9 139.3 %all-reduce.2.cloned.1.call-start = ((), (), s32[]{:S(2)}) async-start(), calls=%async_computation.3 | async-start | bytes 6291456 | tf_op jit(solution)/shard_map/psum | solution.py:85
  120.7 105.0 %reduce-scatter.5.cloned.1.call-start = ((), (), s32[]{:S(2)}) async-start(), calls=%async_computation.4 | async-start | bytes 491520 | tf_op jit(solution)/shard_map/reduce_scatter | solution.py:87
  210.7 15.0 %copy-start.4 = (bf16[96,512]{1,0:T(8,128)(2,1)S(1)}, bf16[96,512]{1,0:T(8,128)(2,1)}, u32[]{:S(2)}) copy-start(bf16[96,512]{1,0:T(8,128)(2,1)} %reduce-scatter.3.cloned.1.call-done) | copy-start | bytes 294916
  210.7 16.5 %copy-start.1 = (bf16[256,4096]{1,0:T(8,128)(2,1)S(1)}, bf16[256,4096]{1,0:T(8,128)(2,1)}, u32[]{:S(2)}) copy-start(bf16[256,4096]{1,0:T(8,128)(2,1)} %param.28) | copy-start | bytes 6291460
Sparse Core Ops, SparseCore 0:
  56.0 33.0 reduce-scatter.2
  120.8 74.3 all-reduce.1
  201.1 24.6 reduce-scatter.4
where the time goes:
time: 235 us; the launch traced here: 234 us
  waiting for transfers between devices  112 us (48%)
  blocking collectives  41.3 us (18%)
  other arithmetic  23.9 us (10%)
  local copies, waits for them, and re-layouts  21.4 us (9%)
  matrix products  20.9 us (9%)
  between operations  13.9 us (6%)
    psum x1, waiting for transfers between devices, local(): up_full = lax.psum(up_part.astype(jnp.bfloat16), 'tp').astype(jnp.float32)  74.3 us
    reduce_scatter x1, waiting for transfers between devices, local(): lax.psum_scatter(partial_value.astype(jnp.bfloat16), 'tp', scatter_dimens...  32.4 us
    unnamed x24, local copies, waits for them, and re-layouts  20.7 us
    all_gather x1, blocking collectives, local(): full_rows = lax.all_gather(tokens, 'tp', axis=1, tiled=True)  17.4 us
    psum x1, blocking collectives, local(): squares = lax.psum(jnp.sum(resid * resid, axis=-1), 'tp')  13.8 us
    all_gather x1, blocking collectives, local(): lax.all_gather(ffn_in, 'kv', axis=0, tiled=True)  10.1 us
    add x1, other arithmetic, local(): matrix = matrix + key_proj[:, :, :, None] * delta[:, :, None, :]  9.81 us
    dot_general x1, matrix products, local(): jnp.dot(hidden, w_down, preferred_element_type=jnp.float32)  5.68 us
  transfers between devices with their start and end apart: 3, of which 3 were waited for; matrix products, arithmetic and copies ran while one was open for 9% of the time, Pallas kernels for 0%

commit v1 on v0

--- a/solution.py
+++ b/solution.py
@@ -82,7 +82,9 @@
     up_part = jnp.dot(
         lax.all_gather(ffn_in, "kv", axis=0, tiled=True), w_up, preferred_element_type=jnp.float32
     )
-    up_full = lax.psum(up_part.astype(jnp.bfloat16), "tp").astype(jnp.float32)
+    up_full = jnp.sum(lax.all_gather(up_part.astype(jnp.bfloat16), "tp"), axis=0).astype(
+        jnp.float32
+    )
     hidden = jnp.square(jax.nn.relu(up_full)).astype(jnp.bfloat16)
     down = lax.psum_scatter(
         jnp.dot(hidden, w_down, preferred_element_type=jnp.float32).astype(jnp.bfloat16),

time: 235 us -> 391 us (1.66)
  waiting for transfers between devices: 112 us -> 254 us
  other arithmetic: 23.9 us -> 39.1 us
    all_gather x0 -> x1, waiting for transfers between devices: none -> 218 us  [local(): lax.all_gather(up_part.astype(jnp.bfloat16), 'tp')]
    psum x1 -> x0, waiting for transfers between devices: 74.3 us -> none  [local(): up_full = lax.psum(up_part.astype(jnp.bfloat16), 'tp').astype(jnp.float32)]
    reduce_sum x0 -> x1, other arithmetic: none -> 15.2 us  [local(): jnp.sum(lax.all_gather(up_part.astype(jnp.bfloat16), 'tp'), axis=0)]
  transfers between devices with their start and end apart: 3 -> 3, of which waited for: 3 -> 3; matrix products, arithmetic and copies ran while one was open for 9% -> 5% of each run, Pallas kernels for 0% -> 0%
where the time goes in v1:
time: 391 us; the launch traced here: 390 us
  waiting for transfers between devices  254 us (65%)
  blocking collectives  41.2 us (11%)
  other arithmetic  39.1 us (10%)
  local copies, waits for them, and re-layouts  21.4 us (5%)
  matrix products  20.9 us (5%)
  between operations  13.9 us (4%)
    all_gather x1, waiting for transfers between devices, local(): lax.all_gather(up_part.astype(jnp.bfloat16), 'tp')  218 us
    reduce_scatter x1, waiting for transfers between devices, local(): lax.psum_scatter(partial_value.astype(jnp.bfloat16), 'tp', scatter_dimens...  32.4 us
    unnamed x24, local copies, waits for them, and re-layouts  20.6 us
    all_gather x1, blocking collectives, local(): full_rows = lax.all_gather(tokens, 'tp', axis=1, tiled=True)  17.4 us
    reduce_sum x1, other arithmetic, local(): jnp.sum(lax.all_gather(up_part.astype(jnp.bfloat16), 'tp'), axis=0)  15.2 us
    psum x1, blocking collectives, local(): squares = lax.psum(jnp.sum(resid * resid, axis=-1), 'tp')  13.8 us
    all_gather x1, blocking collectives, local(): lax.all_gather(ffn_in, 'kv', axis=0, tiled=True)  9.97 us
    add x1, other arithmetic, local(): matrix = matrix + key_proj[:, :, :, None] * delta[:, :, None, :]  9.87 us
  transfers between devices with their start and end apart: 3, of which 3 were waited for; matrix products, arithmetic and copies ran while one was open for 5% of the time, Pallas kernels for 0%

profile of v1, /device:TPU:0, one launch (start us, length us, event | category | flops | bytes accessed | tf_op | source)
XLA Modules:
  0.0 390.5 jit_solution(9699485979794289456)
XLA Ops:
  7.2 0.0 copy-start
  7.2 0.0 reduce-scatter.3.cloned.1.call-start
  7.2 0.8 neg.14
  8.0 17.4 %all_gather.12 = bf16[96,4096]{1,0:T(8,128)(2,1)S(1)} all-gather(bf16[96,512]{1,0:T(8,128)(2,1)} %param.16), channel_id=1, replica_groups=mesh['kv'=4,'tp'=8] {'tp'}, dimensions={1}, use_global_device_ids=true | all-gather | bytes 884736 | tf_op jit(solution)/shard_map/all_gather | solution.py:36
  25.4 0.3 fusion.2
  25.7 2.7 fusion.21
  28.4 0.0 copy-done.6
  28.4 0.0 copy-done.9
  28.4 0.0 copy-start.7
  28.5 1.0 fusion.18
  29.5 0.6 copy-done.7
  30.0 1.0 multiply_reduce_fusion.4
  31.1 0.6 copy-done.8
  31.6 1.0 multiply_reduce_fusion.5
  32.7 0.0 copy-start.10
  32.7 9.1 %copy.22 = f32[96,4,4096]{0,2,1:T(8,128)} copy(f32[96,4,4096]{2,1,0:T(4,128)} %param.17) | data formatting | bytes 12582912 | tf_op args[1]
  41.8 1.2 fusion.8
  43.1 0.0 copy-done.10
  43.1 1.2 fusion.12
  44.3 0.0 copy-start.2
  44.4 5.0 %multiply_reduce_fusion.1 = f32[96,4,64]{0,2,1:T(8,128)S(1)} fusion(f32[96,4,64,64]{0,3,2,1:T(8,128)} %bitcast.22, f32[96,4,64]{0,2,1:T(8,128)S(1)} %broadcast_multiply_fusion.1, f32[96,4]{0,1:T(4,128)S(1)} %fusion.12), kind=kLoop, calls=%fused_computation.2 | loop fusion | flops 4694016 | bytes 6489600 | tf_op jit(solution)/shard_map/bhk,bhkv->bhv/dot_general | solution.py:62
  49.4 0.7 copy-done.2
  50.1 4.2 %broadcast_multiply_fusion = (f32[96,4,64,64]{0,3,2,1:T(8,128)}, f32[96,4,64]{0,2,1:T(8,128)S(1)}) fusion(f32[96,4,64]{0,2,1:T(8,128)S(1)} %get-tuple-element.10, f32[96,4,64]{0,2,1:T(8,128)S(1)} %broadcast_multiply_fusion.1, f32[96,4,64,64]{0,3,2,1:T(8,128)S(1)} %bitcast.23, f32[96,4]{0,1:T(4,128)S(1)} %fusion.12, f32[96,4,64]{0,2,1:T(8,128)S(1)} %get-tuple-element.11), kind=kLoop, calls=%fused_computation.6 | loop fusion | flops 7839744 | bytes 12977664 | tf_op jit(solution)/shard_map/mul | solution.py:64
  54.4 0.0 copy-done.5
  54.4 0.1 multiply_convert_fusion.5
  54.5 0.0 copy-done
  54.5 1.4 convolution_convert_fusion.1
  55.9 0.0 reduce-scatter.3.cloned.1.call-update
  55.9 0.0 all-gather.3.cloned.1.call-start
  55.9 0.8 dynamic_slice.11
  56.7 32.4 %reduce-scatter.3.cloned.1.call-done = bf16[96,512]{1,0:T(8,128)(2,1)} async-done(((bf16[96,4096]{1,0:T(8,128)(2,1)}), bf16[96,512]{1,0:T(8,128)(2,1)}) %reduce-scatter.3.cloned.1.call-update) | async-done | bytes 98320 | tf_op jit(solution)/shard_map/reduce_scatter | solution.py:76
  89.1 0.0 copy-done.3
  89.1 1.0 multiply_reduce_fusion.2
  90.1 13.8 %psum.7 = f32[96]{0:T(128)S(1)} all-reduce(f32[96]{0:T(128)S(1)} %multiply_reduce_fusion.2), channel_id=1, replica_groups=mesh['kv'=4,'tp'=8] {'tp'}, use_global_device_ids=true, to_apply=%region_6.7 | all-reduce | flops 96 | bytes 768 | tf_op jit(solution)/shard_map/psum | solution.py:79
  103.9 1.0 multiply_convert_fusion.4
  104.9 10.0 %all_gather.13 = bf16[384,512]{1,0:T(8,128)(2,1)S(1)} all-gather(bf16[96,512]{1,0:T(8,128)(2,1)S(1)} %multiply_convert_fusion.4), channel_id=1, replica_groups=mesh['kv'=4,'tp'=8] {'kv'}, dimensions={0}, use_global_device_ids=true | all-gather | bytes 491520 | tf_op jit(solution)/shard_map/all_gather | solution.py:83
  114.9 5.7 %convolution_convert_fusion = bf16[384,4096]{1,0:T(8,128)(2,1)} fusion(bf16[384,512]{1,0:T(8,128)(2,1)S(1)} %all_gather.13, bf16[512,4096]{1,0:T(8,128)(2,1)} %param.30), kind=kOutput, calls=%fused_computation.4 | convolution fusion | flops 1612185600 | bytes 7733248 | tf_op jit(solution)/shard_map/dot_general | solution.py:82
  120.5 0.0 all-gather.3.cloned.1.call-update
  120.6 0.2 reduce-scatter.5.cloned.1.call-start
  120.8 217.6 %all-gather.3.cloned.1.call-done = bf16[3072,4096]{1,0:T(8,128)(2,1)} async-done(((bf16[384,4096]{1,0:T(8,128)(2,1)}), bf16[3072,4096]{1,0:T(8,128)(2,1)}) %all-gather.3.cloned.1.call-update) | async-done | bytes 25165840 | tf_op jit(solution)/shard_map/all_gather | solution.py:85
  338.4 15.2 %reduce_sum.62 = bf16[384,4096]{1,0:T(8,128)(2,1)} reduce(bf16[8,384,4096]{2,1,0:T(8,128)(2,1)} %bitcast.24, bf16[]{:T(256)} %constant.37.clone.1), dimensions={0}, to_apply=%region_7.8 | reduce | flops 11010048 | bytes 28311554 | tf_op jit(solution)/shard_map/reduce_sum | solution.py:85
  353.6 5.7 %fusion.5 = bf16[384,512]{1,0:T(8,128)(2,1)} fusion(bf16[4096,512]{1,0:T(8,128)(2,1)} %param.31, bf16[384,4096]{1,0:T(8,128)(2,1)} %reduce_sum.62), kind=kOutput, calls=%fused_computation.14 | convolution fusion | flops 1617100800 | bytes 7733248 | tf_op jit(solution)/shard_map/dot_general | solution.py:90
  359.3 0.0 reduce-scatter.5.cloned.1.call-update
  359.3 9.9 %bitcast_add_fusion = f32[96,4,4096]{0,2,1:T(8,128)} fusion(f32[96,4,64,64]{0,3,2,1:T(8,128)} %get-tuple-element.4, f32[96,4,4096]{0,2,1:T(8,128)} %copy.22, f32[96,4]{0,1:T(4,128)S(1)} %fusion.12), kind=kLoop, calls=%fused_computation | loop fusion | flops 3145728 | bytes 18875904 | tf_op jit(solution)/shard_map/add | solution.py:64
  369.2 9.6 %copy.27 = f32[96,4,4096]{2,1,0:T(4,128)} copy(f32[96,4,4096]{0,2,1:T(8,128)} %bitcast_add_fusion) | data formatting | bytes 12582912
  378.7 3.6 reduce-scatter.5.cloned.1.call-done
  382.4 0.0 copy-done.4
  382.4 1.6 add_convert_fusion
  (16 shorter events, 0.1 us)
Async XLA Ops:
  7.2 47.3 %copy-start = (bf16[256,4096]{1,0:T(8,128)(2,1)S(1)}, bf16[256,4096]{1,0:T(8,128)(2,1)}, u32[]{:S(2)}) copy-start(bf16[256,4096]{1,0:T(8,128)(2,1)} %param.28) | copy-start | bytes 6291460
  7.2 81.9 %reduce-scatter.3.cloned.1.call-start = ((), (), s32[]{:S(2)}) async-start(), calls=%async_computation.2 | async-start | bytes 884736 | tf_op jit(solution)/shard_map/reduce_scatter | solution.py:76
  25.4 3.0 copy-start.6
  25.4 3.0 copy-start.9
  28.4 1.6 copy-start.7
  30.0 1.6 copy-start.8
  32.7 10.4 %copy-start.10 = (f32[4]{0:T(128)S(1)}, f32[4]{0:T(128)}, u32[]{:S(2)}) copy-start(f32[4]{0:T(128)} %param.25) | copy-start | bytes 52
  44.3 5.8 %copy-start.2 = (f32[96,4,4096]{0,2,1:T(8,128)S(1)}, f32[96,4,4096]{0,2,1:T(8,128)}, u32[]{:S(2)}) copy-start(f32[96,4,4096]{0,2,1:T(8,128)} %copy.22) | copy-start | bytes 18874372
  50.1 4.2 %copy-start.5 = (f32[64]{0:T(128)S(1)}, f32[64]{0:T(128)}, u32[]{:S(2)}) copy-start(f32[64]{0:T(128)} %param.27) | copy-start | bytes 772
  54.3 34.8 %copy-start.3 = (bf16[96,512]{1,0:T(8,128)(2,1)S(1)}, bf16[96,512]{1,0:T(8,128)(2,1)}, u32[]{:S(2)}) copy-start(bf16[96,512]{1,0:T(8,128)(2,1)} %param.16) | copy-start | bytes 294916
  55.9 282.5 %all-gather.3.cloned.1.call-start = ((), (), s32[]{:S(2)}) async-start(), calls=%async_computation.4 | async-start | bytes 28311552 | tf_op jit(solution)/shard_map/all_gather | solution.py:85
  120.6 261.8 %reduce-scatter.5.cloned.1.call-start = ((), (), s32[]{:S(2)}) async-start(), calls=%async_computation.3 | async-start | bytes 491520 | tf_op jit(solution)/shard_map/reduce_scatter | solution.py:89
  369.2 13.2 %copy-start.4 = (bf16[96,512]{1,0:T(8,128)(2,1)S(1)}, bf16[96,512]{1,0:T(8,128)(2,1)}, u32[]{:S(2)}) copy-start(bf16[96,512]{1,0:T(8,128)(2,1)} %reduce-scatter.3.cloned.1.call-done) | copy-start | bytes 294916
  369.2 14.8 %copy-start.1 = (bf16[256,4096]{1,0:T(8,128)(2,1)S(1)}, bf16[256,4096]{1,0:T(8,128)(2,1)}, u32[]{:S(2)}) copy-start(bf16[256,4096]{1,0:T(8,128)(2,1)} %param.28) | copy-start | bytes 6291460
Sparse Core Ops, SparseCore 0:
  56.0 33.0 reduce-scatter.2
  120.7 217.6 all-gather.2
  359.4 22.9 reduce-scatter.4
